TPU v7x, 32 devices: a whole 2x2x4 slice. The times are simulated.
32 devices in a mesh: fs: 8 (over z, x), tp: 4 (over y, core).
Axes of the slice: x: 2, y: 2, z: 4, core: 2. Of those that a mesh axis runs over, the one named last changes fastest.
Arguments:
- tokens: bfloat16 [1024, 2048], P('fs', 'tp'), may hold values from -6 to 6
- routes: int32 [1024, 2], P('fs'), may hold values from 0 to 3, all different within a row; in each aligned block of 128 rows (0 to 127, 128 to 255, ...) at most 96 rows name the same one
- route_weight: float32 [1024, 2], P('fs'), may hold values from 0.1 to 1
- norm_gain: float32 [2048], P('fs'), may hold values from 0.1 to 1.9
- expert_gate: float32 [4, 2048, 512], P(None, 'fs', 'tp'), may hold values from -0.125 to 0.125
- expert_up: float32 [4, 2048, 512], P(None, 'fs', 'tp'), may hold values from -0.125 to 0.125
- expert_down: float32 [4, 2048, 512], P(None, 'fs', 'tp'), may hold values from -0.25 to 0.25
- shared_gate: float32 [2048, 512], P('fs', 'tp'), may hold values from -0.125 to 0.125
- shared_up: float32 [2048, 512], P('fs', 'tp'), may hold values from -0.125 to 0.125
- shared_down: float32 [512, 2048], P('tp', 'fs'), may hold values from -0.25 to 0.25
Outputs:
- mixed: bfloat16 [1024, 2048], P('fs', 'tp')
- gate_sampler: bfloat16 [8, 2048, 256], P('fs', None, 'tp')
- up_sampler: bfloat16 [8, 2048, 256], P('fs', None, 'tp')
- down_sampler: bfloat16 [8, 2048, 256], P('fs', 'tp')
- shared_gate_out: bfloat16 [2048, 512], P(None, 'tp')
- shared_up_out: bfloat16 [2048, 512], P(None, 'tp')
- shared_down_out: bfloat16 [512, 2048], P('tp')
Inputs may be any that keep to these rules, and one draw needn't show every extreme that they name: `routes`: each row names 2 different experts. In each aligned block of 128 rows no expert is named by more than 96 rows, a bound that some block reaches.
All inputs are finite; a program needn't handle non-finite values.
Results may differ from a plain program's by a relative error of at most 0.009.
Values may be sent and summed in bfloat16 or wider, within the bound.
No kernel may reach another device: no remote copies, remote signals or barrier semaphores. Data moves between devices by JAX's collectives and lax.ppermute only.
A program may use at most 64 MiB of HBM per device.

v0:
```python
import jax
import jax.numpy as jnp
from jax import lax
from jax.sharding import PartitionSpec as P

EPS = 1e-06


def to_owners(matrix, expert_count, unit_count):
    row_share = matrix.shape[1]
    return (
        matrix.reshape(expert_count, row_share, 2, unit_count)
        .transpose(0, 2, 1, 3)
        .reshape(2 * expert_count, row_share, unit_count)
    )


def on_device(
    tokens,
    routes,
    route_weight,
    norm_gain,
    expert_gate,
    expert_up,
    expert_down,
    shared_gate,
    shared_up,
    shared_down,
):
    fs_count = lax.axis_size("fs")
    tp_count = lax.axis_size("tp")
    expert_count, row_share, col_share = expert_gate.shape
    unit_count = col_share // 2
    model_width = row_share * fs_count
    quarter = model_width // tp_count
    tok_count, pick_count = routes.shape
    capacity = 2 * ((3 * tok_count * pick_count + 4 * expert_count - 1) // (4 * expert_count))
    slot_count = fs_count * capacity
    row_gain = norm_gain[None, :, None]
    gate_owned = to_owners((expert_gate * row_gain).astype(jnp.bfloat16), expert_count, unit_count)
    up_owned = to_owners((expert_up * row_gain).astype(jnp.bfloat16), expert_count, unit_count)
    gate_new, up_new = (
        lax.all_to_all(gate_owned, "fs", split_axis=0, concat_axis=1, tiled=True),
        lax.all_to_all(up_owned, "fs", split_axis=0, concat_axis=1, tiled=True),
    )
    down_owned = to_owners(expert_down.astype(jnp.bfloat16), expert_count, unit_count)
    down_new = lax.all_to_all(
        lax.all_to_all(down_owned, "fs", split_axis=0, concat_axis=1, tiled=True),
        "tp",
        split_axis=1,
        concat_axis=2,
        tiled=True,
    )
    shared_gate_new, shared_up_new, shared_down_new = (
        lax.all_gather(
            (shared_gate * norm_gain[:, None]).astype(jnp.bfloat16), "fs", axis=0, tiled=True
        ),
        lax.all_gather(
            (shared_up * norm_gain[:, None]).astype(jnp.bfloat16), "fs", axis=0, tiled=True
        ),
        lax.all_gather(shared_down.astype(jnp.bfloat16), "fs", axis=1, tiled=True),
    )
    gathered = lax.all_gather(tokens, "tp", axis=1, tiled=True)
    tokens_wide = gathered.astype(jnp.float32)
    normed = (
        tokens_wide * lax.rsqrt(jnp.mean(tokens_wide * tokens_wide, axis=1, keepdims=True) + EPS)
    ).astype(jnp.bfloat16)
    shared_act = jnp.dot(normed, shared_gate_new, preferred_element_type=jnp.float32)
    shared_lin = jnp.dot(normed, shared_up_new, preferred_element_type=jnp.float32)
    shared_hidden = (jax.nn.silu(shared_act) * shared_lin).astype(jnp.bfloat16)
    shared_term = jnp.dot(shared_hidden, shared_down_new, preferred_element_type=jnp.float32)
    shared_sum = lax.psum_scatter(
        shared_term.astype(jnp.bfloat16), "tp", scatter_dimension=1, tiled=True
    ).astype(jnp.float32)
    assigned = routes.reshape(-1)
    onehot = (assigned[:, None] == jnp.arange(expert_count, dtype=jnp.int32)[None, :]).astype(
        jnp.int32
    )
    earlier = jnp.cumsum(onehot, axis=0) - onehot
    position = jnp.sum(earlier * onehot, axis=1)
    slot_index = assigned * capacity + position
    token_index = jnp.arange(tok_count * pick_count, dtype=jnp.int32) // pick_count
    slot_token = (
        jnp.full((expert_count * capacity,), tok_count, jnp.int32).at[slot_index].set(token_index)
    )
    padded = jnp.concatenate([normed, jnp.zeros((1, model_width), jnp.bfloat16)], axis=0)
    own_part = lax.dynamic_slice_in_dim(padded, lax.axis_index("tp") * quarter, quarter, 1)
    outgoing = jnp.repeat(
        own_part[slot_token].reshape(expert_count, capacity, quarter), 2, axis=0
    ).reshape(slot_count, quarter)
    arrived = lax.all_to_all(outgoing, "fs", split_axis=0, concat_axis=0, tiled=True)
    portion = lax.all_gather(arrived, "tp", axis=1, tiled=True)
    gate_rows = gate_new[0]
    up_rows = up_new[0]
    gate_act = jnp.dot(portion, gate_rows, preferred_element_type=jnp.float32)
    up_act = jnp.dot(portion, up_rows, preferred_element_type=jnp.float32)
    hidden = (jax.nn.silu(gate_act) * up_act).astype(jnp.bfloat16)
    down_cols = down_new[0]
    half_sum = lax.dot_general(
        lax.all_gather(hidden, "tp", axis=1, tiled=True),
        down_cols,
        (((1,), (1,)), ((), ())),
        preferred_element_type=jnp.float32,
    )
    returned = lax.all_to_all(
        half_sum.astype(jnp.bfloat16), "fs", split_axis=0, concat_axis=0, tiled=True
    )
    pair_sum = jnp.sum(
        returned.astype(jnp.float32).reshape(expert_count, 2, capacity, quarter), axis=1
    ).reshape(expert_count * capacity, quarter)
    gathered_slots = pair_sum[slot_index].reshape(tok_count, pick_count, quarter)
    routed = jnp.sum(gathered_slots * route_weight[:, :, None], axis=1)
    mixed = (shared_sum + routed).astype(jnp.bfloat16)
    return (mixed, gate_new, up_new, down_new, shared_gate_new, shared_up_new, shared_down_new)


def solution(mesh):
    in_specs = (
        P("fs", "tp"),
        P("fs", None),
        P("fs", None),
        P("fs"),
        P(None, "fs", "tp"),
        P(None, "fs", "tp"),
        P(None, "fs", "tp"),
        P("fs", "tp"),
        P("fs", "tp"),
        P("tp", "fs"),
    )
    out_specs = (
        P("fs", "tp"),
        P("fs", None, "tp"),
        P("fs", None, "tp"),
        P("fs", "tp", None),
        P(None, "tp"),
        P(None, "tp"),
        P("tp", None),
    )
    return jax.shard_map(
        on_device, mesh=mesh, in_specs=in_specs, out_specs=out_specs, check_vma=False
    )
```

profile of v0, /device:TPU:0, one launch (start us, length us, event | category | flops | bytes accessed | tf_op | source)
XLA Modules:
  0.0 257.9 jit_solution(7877371888522557811)
XLA Ops:
  9.0 8.9 %all_gather.18 = bf16[128,2048]{1,0:T(8,128)(2,1)S(1)} all-gather(bf16[128,512]{1,0:T(8,128)(2,1)} %param.10), channel_id=1, replica_groups=mesh['fs'=8,'tp'=4] {'tp'}, dimensions={1}, use_global_device_ids=true | all-gather | bytes 655360 | tf_op jit(solution)/shard_map/all_gather | solution.py:63
  18.2 1.2 reduce-window.6
  20.1 1.4 scatter_custom_fusion
  21.6 2.1 gather_fusion
  23.8 26.3 %all_to_all.75 = bf16[8,96,512]{2,1,0:T(8,128)(2,1)} all-to-all(bf16[8,96,512]{2,1,0:T(8,128)(2,1)S(1)} %bitcast.62), channel_id=1, replica_groups=mesh['fs'=8,'tp'=4] {'fs'}, dimensions={0} | all-to-all | bytes 1572864 | tf_op jit(solution)/shard_map/all_to_all | solution.py:91
  51.6 3.6 %all-to-all-start.1 = ((bf16[8,256,64]{1,2,0:T(8,128)(2,1)}), bf16[8,256,64]{1,2,0:T(8,128)(2,1)S(1)}, u32[]{:S(2)}, u32[]{:S(2)}) async-start(bf16[8,256,64]{1,2,0:T(8,128)(2,1)} %copy.50), calls=%async_computation.2 | async-start | bytes 524288 | tf_op jit(solution)/shard_map/all_to_all | solution.py:43
  56.4 7.8 %all-to-all-done.1 = bf16[8,256,64]{1,2,0:T(8,128)(2,1)S(1)} async-done(((bf16[8,256,64]{1,2,0:T(8,128)(2,1)}), bf16[8,256,64]{1,2,0:T(8,128)(2,1)S(1)}, u32[]{:S(2)}, u32[]{:S(2)}) %all-to-all-start.1) | async-done | bytes 262176 | tf_op jit(solution)/shard_map/all_to_all | solution.py:43
  64.2 3.6 %all-to-all-start.3 = ((bf16[8,256,64]{1,2,0:T(8,128)(2,1)}), bf16[8,256,64]{1,2,0:T(8,128)(2,1)S(1)}, u32[]{:S(2)}, u32[]{:S(2)}) async-start(bf16[8,256,64]{1,2,0:T(8,128)(2,1)} %copy.56), calls=%async_computation.4 | async-start | bytes 524288 | tf_op jit(solution)/shard_map/all_to_all | solution.py:48
  68.8 7.6 %all-to-all-done.3 = bf16[8,256,64]{1,2,0:T(8,128)(2,1)S(1)} async-done(((bf16[8,256,64]{1,2,0:T(8,128)(2,1)}), bf16[8,256,64]{1,2,0:T(8,128)(2,1)S(1)}, u32[]{:S(2)}, u32[]{:S(2)}) %all-to-all-start.3) | async-done | bytes 262176 | tf_op jit(solution)/shard_map/all_to_all | solution.py:48
  76.4 3.6 %all-to-all-start.2 = ((bf16[8,256,64]{1,2,0:T(8,128)(2,1)}), bf16[8,256,64]{1,2,0:T(8,128)(2,1)S(1)}, u32[]{:S(2)}, u32[]{:S(2)}) async-start(bf16[8,256,64]{1,2,0:T(8,128)(2,1)} %copy.53), calls=%async_computation.3 | async-start | bytes 524288 | tf_op jit(solution)/shard_map/all_to_all | solution.py:44
  80.1 33.5 %all_gather.19 = bf16[2048,128]{1,0:T(8,128)(2,1)S(1)} all-gather(bf16[256,128]{1,0:T(8,128)(2,1)S(1)} %get-tuple-element.34), channel_id=1, replica_groups=mesh['fs'=8,'tp'=4] {'fs'}, dimensions={0}, use_global_device_ids=true | all-gather | bytes 589824 | tf_op jit(solution)/shard_map/all_gather | solution.py:55
  114.7 11.5 %reduce = bf16[2048,64]{1,0:T(8,128)(2,1)S(1)} reduce(bf16[2048,1,64]{2,1,0:T(2,128)(2,1)S(1)} %bitcast.60, bf16[]{:T(256)} %broadcast.90), dimensions={1}, to_apply=%bitcast.45.reduce_sub_computation | reduce | bytes 524290
  126.2 1.1 reshape.151
  127.3 3.4 %all-to-all-start.4 = ((bf16[4,2,16384]{2,1,0:T(2,128)(2,1)}), bf16[4,2,16384]{2,1,0:T(2,128)(2,1)S(1)}, u32[]{:S(2)}, u32[]{:S(2)}) async-start(bf16[4,2,16384]{2,1,0:T(2,128)(2,1)} %reshape.151), calls=%async_computation.5 | async-start | bytes 524288 | tf_op jit(solution)/shard_map/all_to_all | solution.py:47
  130.8 31.5 %all_gather.20 = bf16[2048,128]{1,0:T(8,128)(2,1)S(1)} all-gather(bf16[256,128]{1,0:T(8,128)(2,1)S(1)} %get-tuple-element.35), channel_id=1, replica_groups=mesh['fs'=8,'tp'=4] {'fs'}, dimensions={0}, use_global_device_ids=true | all-gather | bytes 589824 | tf_op jit(solution)/shard_map/all_gather | solution.py:58
  165.3 3.1 %fusion.20 = f32[768,64]{0,1:T(8,128)S(1)} fusion(bf16[768,2048]{1,0:T(8,128)(2,1)} %all-gather.2.cloned.1.call-done, bf16[2048,64]{0,1:T(8,128)(2,1)} %bitcast.71), kind=kOutput, calls=%fused_computation.54 | convolution fusion | flops 201326592 | bytes 3604480 | tf_op jit(solution)/shard_map/dot_general | solution.py:95
  169.5 7.3 %all_gather.23 = bf16[768,256]{0,1:T(8,128)(2,1)S(1)} all-gather(bf16[768,64]{0,1:T(8,128)(2,1)S(1)} %fusion), channel_id=1, replica_groups=mesh['fs'=8,'tp'=4] {'tp'}, dimensions={1}, use_global_device_ids=true | all-gather | bytes 491520 | tf_op jit(solution)/shard_map/all_gather | solution.py:100
  176.7 1.3 convolution_convert_fusion.1
  178.0 4.3 %all-to-all-start.5 = ((bf16[8,96,512]{2,1,0:T(8,128)(2,1)}), bf16[8,96,512]{2,1,0:T(8,128)(2,1)}, u32[]{:S(2)}, u32[]{:S(2)}) async-start(bf16[8,96,512]{2,1,0:T(8,128)(2,1)} %bitcast.12), calls=%async_computation.6 | async-start | bytes 1572864 | tf_op jit(solution)/shard_map/all_to_all | solution.py:105
  182.4 43.3 %all_gather.21 = bf16[128,2048]{1,0:T(8,128)(2,1)S(1)} all-gather(bf16[128,256]{1,0:T(8,128)(2,1)S(1)} %convert_element_type.61), channel_id=1, replica_groups=mesh['fs'=8,'tp'=4] {'fs'}, dimensions={1}, use_global_device_ids=true | all-gather | bytes 589824 | tf_op jit(solution)/shard_map/all_gather | solution.py:61
  226.0 1.3 convolution_convert_fusion
  230.3 1.4 convert_reduce_fusion
  233.7 13.4 %reduce-scatter.2.cloned.1.call-done = bf16[128,512]{1,0:T(8,128)(2,1)} async-done(((bf16[128,2048]{1,0:T(8,128)(2,1)}), bf16[128,512]{1,0:T(8,128)(2,1)}) %reduce-scatter.2.cloned.1.call-update) | async-done | bytes 131088 | tf_op jit(solution)/shard_map/reduce_scatter | solution.py:72
  247.1 1.6 add_convert_fusion
  (87 shorter events, 19.3 us)
Async XLA Ops:
  7.2 158.1 %all-gather.2.cloned.1.call-start = ((), (), s32[]{:S(2)}) async-start(), calls=%async_computation.8 | async-start | bytes 3932160 | tf_op jit(solution)/shard_map/all_gather | solution.py:92
  21.6 28.5 %copy-start.2 = (f32[4,256,128]{2,1,0:T(8,128)S(1)}, f32[4,256,128]{2,1,0:T(8,128)}, u32[]{:S(2)}) copy-start(f32[4,256,128]{2,1,0:T(8,128)} %param.14) | copy-start | bytes 1572868
  21.6 28.5 %copy-start.3 = (f32[4,256,128]{2,1,0:T(8,128)S(1)}, f32[4,256,128]{2,1,0:T(8,128)}, u32[]{:S(2)}) copy-start(f32[4,256,128]{2,1,0:T(8,128)} %param.15) | copy-start | bytes 1572868
  21.6 28.5 %copy-start.8 = (f32[256]{0:T(256)S(1)}, f32[256]{0:T(256)}, u32[]{:S(2)}) copy-start(f32[256]{0:T(256)} %param.13) | copy-start | bytes 3076
  50.1 5.1 %copy-start.1 = (f32[4,256,128]{2,1,0:T(8,128)S(1)}, f32[4,256,128]{2,1,0:T(8,128)}, u32[]{:S(2)}) copy-start(f32[4,256,128]{2,1,0:T(8,128)} %param.16) | copy-start | bytes 1572868
  51.6 12.6 %all-to-all-start.1 = ((bf16[8,256,64]{1,2,0:T(8,128)(2,1)}), bf16[8,256,64]{1,2,0:T(8,128)(2,1)S(1)}, u32[]{:S(2)}, u32[]{:S(2)}) async-start(bf16[8,256,64]{1,2,0:T(8,128)(2,1)} %copy.50), calls=%async_computation.2 | async-start | bytes 524288 | tf_op jit(solution)/shard_map/all_to_all | solution.py:43
  55.2 13.6 %copy-start.7 = (f32[128,256]{1,0:T(8,128)S(1)}, f32[128,256]{1,0:T(8,128)}, u32[]{:S(2)}) copy-start(f32[128,256]{1,0:T(8,128)} %param.19) | copy-start | bytes 393220
  55.3 24.8 %copy-start.5 = (f32[256,128]{1,0:T(8,128)S(1)}, f32[256,128]{1,0:T(8,128)}, u32[]{:S(2)}) copy-start(f32[256,128]{1,0:T(8,128)} %param.17) | copy-start | bytes 393220
  55.3 24.7 %copy-start.6 = (f32[256,128]{1,0:T(8,128)S(1)}, f32[256,128]{1,0:T(8,128)}, u32[]{:S(2)}) copy-start(f32[256,128]{1,0:T(8,128)} %param.18) | copy-start | bytes 393220
  64.2 12.2 %all-to-all-start.3 = ((bf16[8,256,64]{1,2,0:T(8,128)(2,1)}), bf16[8,256,64]{1,2,0:T(8,128)(2,1)S(1)}, u32[]{:S(2)}, u32[]{:S(2)}) async-start(bf16[8,256,64]{1,2,0:T(8,128)(2,1)} %copy.56), calls=%async_computation.4 | async-start | bytes 524288 | tf_op jit(solution)/shard_map/all_to_all | solution.py:48
  76.4 50.9 %all-to-all-start.2 = ((bf16[8,256,64]{1,2,0:T(8,128)(2,1)}), bf16[8,256,64]{1,2,0:T(8,128)(2,1)S(1)}, u32[]{:S(2)}, u32[]{:S(2)}) async-start(bf16[8,256,64]{1,2,0:T(8,128)(2,1)} %copy.53), calls=%async_computation.3 | async-start | bytes 524288 | tf_op jit(solution)/shard_map/all_to_all | solution.py:44
  127.3 36.4 %all-to-all-start.4 = ((bf16[4,2,16384]{2,1,0:T(2,128)(2,1)}), bf16[4,2,16384]{2,1,0:T(2,128)(2,1)S(1)}, u32[]{:S(2)}, u32[]{:S(2)}) async-start(bf16[4,2,16384]{2,1,0:T(2,128)(2,1)} %reshape.151), calls=%async_computation.5 | async-start | bytes 524288 | tf_op jit(solution)/shard_map/all_to_all | solution.py:47
  165.0 3.4 %copy-start.4 = (bf16[8,8,8,256]{3,2,0,1:T(8,128)(2,1)S(1)}, bf16[8,8,8,256]{3,2,0,1:T(8,128)(2,1)}, u32[]{:S(2)}) copy-start(bf16[8,8,8,256]{3,2,0,1:T(8,128)(2,1)} %copy.75) | copy-start | bytes 786436
  165.2 3.1 %copy-start = (bf16[768,2048]{1,0:T(8,128)(2,1)S(1)}, bf16[768,2048]{1,0:T(8,128)(2,1)}, u32[]{:S(2)}) copy-start(bf16[768,2048]{1,0:T(8,128)(2,1)} %all-gather.2.cloned.1.call-done) | copy-start | bytes 9437188
  178.0 49.4 %copy-start.9 = (f32[128,2]{0,1:T(2,128)S(1)}, f32[128,2]{0,1:T(2,128)}, u32[]{:S(2)}) copy-start(f32[128,2]{0,1:T(2,128)} %param.12) | copy-start | bytes 3076
  178.0 52.3 %all-to-all-start.5 = ((bf16[8,96,512]{2,1,0:T(8,128)(2,1)}), bf16[8,96,512]{2,1,0:T(8,128)(2,1)}, u32[]{:S(2)}, u32[]{:S(2)}) async-start(bf16[8,96,512]{2,1,0:T(8,128)(2,1)} %bitcast.12), calls=%async_computation.6 | async-start | bytes 1572864 | tf_op jit(solution)/shard_map/all_to_all | solution.py:105
  182.4 64.7 %reduce-scatter.2.cloned.1.call-start = ((), (), s32[]{:S(2)}) async-start(), calls=%async_computation.7 | async-start | bytes 655360 | tf_op jit(solution)/shard_map/reduce_scatter | solution.py:72
Sparse Core Ops, SparseCore 0:
  50.2 27.1 all-gather.1
  227.5 19.5 reduce-scatter.1
where the time goes:
time: 259 us; the launch traced here: 258 us
  blocking collectives  151 us (58%)
  waiting for transfers between devices  28.8 us (11%)
  local copies, waits for them, and re-layouts  19.9 us (8%)
  starting transfers between devices  18.7 us (7%)
  other arithmetic  18.2 us (7%)
  between operations  14.4 us (6%)
  matrix products  7.12 us (3%)
    all_gather x1, blocking collectives, on_device(): lax.all_gather(shared_down.astype(jnp.bfloat16), 'fs', axis=1, tiled=True)  43.3 us
    all_gather x1, blocking collectives, on_device(): lax.all_gather((shared_gate * norm_gain[:, None]).astype(jnp.bfloat16), '...  33.5 us
    all_gather x1, blocking collectives, on_device(): lax.all_gather((shared_up * norm_gain[:, None]).astype(jnp.bfloat16), 'fs...  31.5 us
    all_to_all x1, blocking collectives, on_device(): lax.all_to_all(outgoing, 'fs', split_axis=0, concat_axis=0, tiled=True)  26.3 us
    reduce_scatter x1, waiting for transfers between devices, on_device(): lax.psum_scatter(shared_term.astype(jnp.bfloat16), 'tp', scatter_dimensio...  13.4 us
    unnamed x2, other arithmetic  11.6 us
    all_gather x1, blocking collectives, on_device(): gathered = lax.all_gather(tokens, 'tp', axis=1, tiled=True)  8.87 us
    all_to_all x1, waiting for transfers between devices, on_device(): lax.all_to_all(gate_owned, 'fs', split_axis=0, concat_axis=1, tiled=True)  7.75 us
  transfers between devices with their start and end apart: 7, of which 3 were waited for; matrix products, arithmetic and copies ran while one was open for 10% of the time, Pallas kernels for 0%

commit v1 on v0

--- a/solution.py
+++ b/solution.py
@@ -27,6 +27,13 @@
     shared_up,
     shared_down,
 ):
+
+    def use_runs(vec, mesh_name):
+        return jnp.concatenate(
+            lax.all_to_all(jnp.stack(jnp.split(vec, lax.axis_size(mesh_name), 1)), mesh_name, 0, 0),
+            2,
+        )
+
     fs_count = lax.axis_size("fs")
     tp_count = lax.axis_size("tp")
     expert_count, row_share, col_share = expert_gate.shape
@@ -44,12 +51,8 @@
         lax.all_to_all(up_owned, "fs", split_axis=0, concat_axis=1, tiled=True),
     )
     down_owned = to_owners(expert_down.astype(jnp.bfloat16), expert_count, unit_count)
-    down_new = lax.all_to_all(
-        lax.all_to_all(down_owned, "fs", split_axis=0, concat_axis=1, tiled=True),
-        "tp",
-        split_axis=1,
-        concat_axis=2,
-        tiled=True,
+    down_new = use_runs(
+        lax.all_to_all(down_owned, "fs", split_axis=0, concat_axis=1, tiled=True), "tp"
     )
     shared_gate_new, shared_up_new, shared_down_new = (
         lax.all_gather(

time: 259 us -> 243 us (0.938)
  other arithmetic: 18.2 us -> 7.43 us
  local copies, waits for them, and re-layouts: 19.9 us -> 15.1 us
    unnamed x2 -> x1, other arithmetic: 11.6 us -> 0.07 us
    all_to_all x1, waiting for transfers between devices: 7.58 us -> 0.01 us  [on_device(): lax.all_to_all(down_owned, 'fs', split_axis=0, concat_axis=1, tiled=True)]
    all_to_all x1, waiting for transfers between devices: 0.01 us -> 7.31 us  [on_device(): lax.all_to_all(up_owned, 'fs', split_axis=0, concat_axis=1, tiled=True)]
    unnamed x29 -> x24, local copies, waits for them, and re-layouts: 6.41 us -> 4.17 us
  transfers between devices with their start and end apart: 7 -> 7, of which waited for: 3 -> 3; matrix products, arithmetic and copies ran while one was open for 10% -> 6% of each run, Pallas kernels for 0% -> 0%
where the time goes in v1:
time: 243 us; the launch traced here: 242 us
  blocking collectives  151 us (62%)
  waiting for transfers between devices  28.9 us (12%)
  starting transfers between devices  18.7 us (8%)
  local copies, waits for them, and re-layouts  15.1 us (6%)
  between operations  14.4 us (6%)
  other arithmetic  7.43 us (3%)
  matrix products  7.1 us (3%)
    all_gather x1, blocking collectives, on_device(): lax.all_gather(shared_down.astype(jnp.bfloat16), 'fs', axis=1, tiled=True)  43.3 us
    all_gather x1, blocking collectives, on_device(): lax.all_gather((shared_gate * norm_gain[:, None]).astype(jnp.bfloat16), '...  33.7 us
    all_gather x1, blocking collectives, on_device(): lax.all_gather((shared_up * norm_gain[:, None]).astype(jnp.bfloat16), 'fs...  31.5 us
    all_to_all x1, blocking collectives, on_device(): lax.all_to_all(outgoing, 'fs', split_axis=0, concat_axis=0, tiled=True)  26.3 us
    reduce_scatter x1, waiting for transfers between devices, on_device(): lax.psum_scatter(shared_term.astype(jnp.bfloat16), 'tp', scatter_dimensio...  13.6 us
    all_gather x1, blocking collectives, on_device(): gathered = lax.all_gather(tokens, 'tp', axis=1, tiled=True)  8.87 us
    all_to_all x1, waiting for transfers between devices, on_device(): lax.all_to_all(gate_owned, 'fs', split_axis=0, concat_axis=1, tiled=True)  7.91 us
    all_to_all x1, waiting for transfers between devices, on_device(): lax.all_to_all(up_owned, 'fs', split_axis=0, concat_axis=1, tiled=True)  7.31 us
  transfers between devices with their start and end apart: 7, of which 3 were waited for; matrix products, arithmetic and copies ran while one was open for 6% of the time, Pallas kernels for 0%

profile of v1, /device:TPU:0, one launch (start us, length us, event | category | flops | bytes accessed | tf_op | source)
XLA Modules:
  0.0 242.2 jit_solution(6645416624748768437)
XLA Ops:
  9.0 8.9 %all_gather.18 = bf16[128,2048]{1,0:T(8,128)(2,1)S(1)} all-gather(bf16[128,512]{1,0:T(8,128)(2,1)} %param.10), channel_id=1, replica_groups=mesh['fs'=8,'tp'=4] {'tp'}, dimensions={1}, use_global_device_ids=true | all-gather | bytes 655360 | tf_op jit(solution)/shard_map/all_gather | solution.py:66
  18.2 1.2 reduce-window.6
  20.1 1.4 scatter_custom_fusion
  21.6 2.1 gather_fusion
  23.8 26.3 %all_to_all.62 = bf16[8,96,512]{2,1,0:T(8,128)(2,1)} all-to-all(bf16[8,96,512]{2,1,0:T(8,128)(2,1)S(1)} %bitcast.68), channel_id=1, replica_groups=mesh['fs'=8,'tp'=4] {'fs'}, dimensions={0} | all-to-all | bytes 1572864 | tf_op jit(solution)/shard_map/all_to_all | solution.py:94
  51.6 3.6 %all-to-all-start.1 = ((bf16[8,256,64]{1,2,0:T(8,128)(2,1)}), bf16[8,256,64]{1,2,0:T(8,128)(2,1)S(1)}, u32[]{:S(2)}, u32[]{:S(2)}) async-start(bf16[8,256,64]{1,2,0:T(8,128)(2,1)} %copy.49), calls=%async_computation.2 | async-start | bytes 524288 | tf_op jit(solution)/shard_map/all_to_all | solution.py:50
  56.3 7.9 %all-to-all-done.1 = bf16[8,256,64]{1,2,0:T(8,128)(2,1)S(1)} async-done(((bf16[8,256,64]{1,2,0:T(8,128)(2,1)}), bf16[8,256,64]{1,2,0:T(8,128)(2,1)S(1)}, u32[]{:S(2)}, u32[]{:S(2)}) %all-to-all-start.1) | async-done | bytes 262176 | tf_op jit(solution)/shard_map/all_to_all | solution.py:50
  64.2 3.6 %all-to-all-start.2 = ((bf16[8,256,64]{1,2,0:T(8,128)(2,1)}), bf16[8,256,64]{1,2,0:T(8,128)(2,1)S(1)}, u32[]{:S(2)}, u32[]{:S(2)}) async-start(bf16[8,256,64]{1,2,0:T(8,128)(2,1)} %copy.52), calls=%async_computation.3 | async-start | bytes 524288 | tf_op jit(solution)/shard_map/all_to_all | solution.py:51
  69.1 7.3 %all-to-all-done.2 = bf16[8,256,64]{1,2,0:T(8,128)(2,1)S(1)} async-done(((bf16[8,256,64]{1,2,0:T(8,128)(2,1)}), bf16[8,256,64]{1,2,0:T(8,128)(2,1)S(1)}, u32[]{:S(2)}, u32[]{:S(2)}) %all-to-all-start.2) | async-done | bytes 262176 | tf_op jit(solution)/shard_map/all_to_all | solution.py:51
  76.4 3.6 %all-to-all-start.3 = ((bf16[8,256,64]{1,2,0:T(8,128)(2,1)}), bf16[8,256,64]{1,2,0:T(8,128)(2,1)S(1)}, u32[]{:S(2)}, u32[]{:S(2)}) async-start(bf16[8,256,64]{1,2,0:T(8,128)(2,1)} %copy.55), calls=%async_computation.4 | async-start | bytes 524288 | tf_op jit(solution)/shard_map/all_to_all | solution.py:55
  80.0 33.7 %all_gather.19 = bf16[2048,128]{1,0:T(8,128)(2,1)S(1)} all-gather(bf16[256,128]{1,0:T(8,128)(2,1)S(1)} %get-tuple-element.38), channel_id=1, replica_groups=mesh['fs'=8,'tp'=4] {'fs'}, dimensions={0}, use_global_device_ids=true | all-gather | bytes 589824 | tf_op jit(solution)/shard_map/all_gather | solution.py:58
  113.7 31.5 %all_gather.20 = bf16[2048,128]{1,0:T(8,128)(2,1)S(1)} all-gather(bf16[256,128]{1,0:T(8,128)(2,1)S(1)} %get-tuple-element.39), channel_id=1, replica_groups=mesh['fs'=8,'tp'=4] {'fs'}, dimensions={0}, use_global_device_ids=true | all-gather | bytes 589824 | tf_op jit(solution)/shard_map/all_gather | solution.py:61
  146.3 3.4 %all-to-all-start.4 = ((bf16[4,1,512,64]{2,3,1,0:T(8,128)(2,1)}), bf16[4,1,512,64]{2,3,1,0:T(8,128)(2,1)S(1)}, u32[]{:S(2)}, u32[]{:S(2)}) async-start(bf16[4,1,512,64]{2,3,1,0:T(8,128)(2,1)} %pad_maximum_fusion.3), calls=%async_computation.5 | async-start | bytes 524288 | tf_op jit(solution)/shard_map/all_to_all | solution.py:33
  149.7 3.1 %fusion.20 = f32[768,64]{0,1:T(8,128)S(1)} fusion(bf16[768,2048]{1,0:T(8,128)(2,1)} %all-gather.2.cloned.1.call-done, bf16[2048,64]{0,1:T(8,128)(2,1)S(1)} %bitcast.77), kind=kOutput, calls=%fused_computation.59 | convolution fusion | flops 201326592 | bytes 3604480 | tf_op jit(solution)/shard_map/dot_general | solution.py:98
  152.9 1.1 fusion
  153.9 6.9 %all_gather.23 = bf16[768,256]{0,1:T(8,128)(2,1)S(1)} all-gather(bf16[768,64]{0,1:T(8,128)(2,1)S(1)} %fusion), channel_id=1, replica_groups=mesh['fs'=8,'tp'=4] {'tp'}, dimensions={1}, use_global_device_ids=true | all-gather | bytes 491520 | tf_op jit(solution)/shard_map/all_gather | solution.py:103
  160.9 1.3 convolution_convert_fusion.1
  162.2 4.3 %all-to-all-start.5 = ((bf16[8,96,512]{2,1,0:T(8,128)(2,1)}), bf16[8,96,512]{2,1,0:T(8,128)(2,1)}, u32[]{:S(2)}, u32[]{:S(2)}) async-start(bf16[8,96,512]{2,1,0:T(8,128)(2,1)} %bitcast.16), calls=%async_computation.6 | async-start | bytes 1572864 | tf_op jit(solution)/shard_map/all_to_all | solution.py:108
  166.6 43.3 %all_gather.21 = bf16[128,2048]{1,0:T(8,128)(2,1)S(1)} all-gather(bf16[128,256]{1,0:T(8,128)(2,1)S(1)} %convert_element_type.61), channel_id=1, replica_groups=mesh['fs'=8,'tp'=4] {'fs'}, dimensions={1}, use_global_device_ids=true | all-gather | bytes 589824 | tf_op jit(solution)/shard_map/all_gather | solution.py:64
  210.2 1.3 convolution_convert_fusion
  214.5 1.4 convert_reduce_fusion
  215.8 1.0 gather_fusion.1
  217.8 13.6 %reduce-scatter.2.cloned.1.call-done = bf16[128,512]{1,0:T(8,128)(2,1)} async-done(((bf16[128,2048]{1,0:T(8,128)(2,1)}), bf16[128,512]{1,0:T(8,128)(2,1)}) %reduce-scatter.2.cloned.1.call-update) | async-done | bytes 131088 | tf_op jit(solution)/shard_map/reduce_scatter | solution.py:75
  231.4 1.6 add_convert_fusion
  (80 shorter events, 14.4 us)
Async XLA Ops:
  7.2 142.5 %all-gather.2.cloned.1.call-start = ((), (), s32[]{:S(2)}) async-start(), calls=%async_computation.8 | async-start | bytes 3932160 | tf_op jit(solution)/shard_map/all_gather | solution.py:95
  21.6 28.5 %copy-start.2 = (f32[4,256,128]{2,1,0:T(8,128)S(1)}, f32[4,256,128]{2,1,0:T(8,128)}, u32[]{:S(2)}) copy-start(f32[4,256,128]{2,1,0:T(8,128)} %param.14) | copy-start | bytes 1572868
  21.6 28.5 %copy-start.3 = (f32[4,256,128]{2,1,0:T(8,128)S(1)}, f32[4,256,128]{2,1,0:T(8,128)}, u32[]{:S(2)}) copy-start(f32[4,256,128]{2,1,0:T(8,128)} %param.15) | copy-start | bytes 1572868
  21.6 28.5 %copy-start.7 = (f32[256]{0:T(256)S(1)}, f32[256]{0:T(256)}, u32[]{:S(2)}) copy-start(f32[256]{0:T(256)} %param.13) | copy-start | bytes 3076
  50.3 5.9 %copy-start.1 = (f32[4,256,128]{2,1,0:T(8,128)S(1)}, f32[4,256,128]{2,1,0:T(8,128)}, u32[]{:S(2)}) copy-start(f32[4,256,128]{2,1,0:T(8,128)} %param.16) | copy-start | bytes 1572868
  51.6 12.6 %all-to-all-start.1 = ((bf16[8,256,64]{1,2,0:T(8,128)(2,1)}), bf16[8,256,64]{1,2,0:T(8,128)(2,1)S(1)}, u32[]{:S(2)}, u32[]{:S(2)}) async-start(bf16[8,256,64]{1,2,0:T(8,128)(2,1)} %copy.49), calls=%async_computation.2 | async-start | bytes 524288 | tf_op jit(solution)/shard_map/all_to_all | solution.py:50
  55.2 13.8 %copy-start.6 = (f32[128,256]{1,0:T(8,128)S(1)}, f32[128,256]{1,0:T(8,128)}, u32[]{:S(2)}) copy-start(f32[128,256]{1,0:T(8,128)} %param.19) | copy-start | bytes 393220
  55.2 13.8 %copy-start.4 = (f32[256,128]{1,0:T(8,128)S(1)}, f32[256,128]{1,0:T(8,128)}, u32[]{:S(2)}) copy-start(f32[256,128]{1,0:T(8,128)} %param.17) | copy-start | bytes 393220
  55.2 13.8 %copy-start.5 = (f32[256,128]{1,0:T(8,128)S(1)}, f32[256,128]{1,0:T(8,128)}, u32[]{:S(2)}) copy-start(f32[256,128]{1,0:T(8,128)} %param.18) | copy-start | bytes 393220
  64.2 12.2 %all-to-all-start.2 = ((bf16[8,256,64]{1,2,0:T(8,128)(2,1)}), bf16[8,256,64]{1,2,0:T(8,128)(2,1)S(1)}, u32[]{:S(2)}, u32[]{:S(2)}) async-start(bf16[8,256,64]{1,2,0:T(8,128)(2,1)} %copy.52), calls=%async_computation.3 | async-start | bytes 524288 | tf_op jit(solution)/shard_map/all_to_all | solution.py:51
  76.4 68.8 %all-to-all-start.3 = ((bf16[8,256,64]{1,2,0:T(8,128)(2,1)}), bf16[8,256,64]{1,2,0:T(8,128)(2,1)S(1)}, u32[]{:S(2)}, u32[]{:S(2)}) async-start(bf16[8,256,64]{1,2,0:T(8,128)(2,1)} %copy.55), calls=%async_computation.4 | async-start | bytes 524288 | tf_op jit(solution)/shard_map/all_to_all | solution.py:55
  146.3 14.6 %all-to-all-start.4 = ((bf16[4,1,512,64]{2,3,1,0:T(8,128)(2,1)}), bf16[4,1,512,64]{2,3,1,0:T(8,128)(2,1)S(1)}, u32[]{:S(2)}, u32[]{:S(2)}) async-start(bf16[4,1,512,64]{2,3,1,0:T(8,128)(2,1)} %pad_maximum_fusion.3), calls=%async_computation.5 | async-start | bytes 524288 | tf_op jit(solution)/shard_map/all_to_all | solution.py:33
  149.7 3.1 %copy-start = (bf16[768,2048]{1,0:T(8,128)(2,1)S(1)}, bf16[768,2048]{1,0:T(8,128)(2,1)}, u32[]{:S(2)}) copy-start(bf16[768,2048]{1,0:T(8,128)(2,1)} %all-gather.2.cloned.1.call-done) | copy-start | bytes 9437188
  162.2 49.4 %copy-start.8 = (f32[128,2]{0,1:T(2,128)S(1)}, f32[128,2]{0,1:T(2,128)}, u32[]{:S(2)}) copy-start(f32[128,2]{0,1:T(2,128)} %param.12) | copy-start | bytes 3076
  162.2 52.3 %all-to-all-start.5 = ((bf16[8,96,512]{2,1,0:T(8,128)(2,1)}), bf16[8,96,512]{2,1,0:T(8,128)(2,1)}, u32[]{:S(2)}, u32[]{:S(2)}) async-start(bf16[8,96,512]{2,1,0:T(8,128)(2,1)} %bitcast.16), calls=%async_computation.6 | async-start | bytes 1572864 | tf_op jit(solution)/shard_map/all_to_all | solution.py:108
  166.5 64.9 %reduce-scatter.2.cloned.1.call-start = ((), (), s32[]{:S(2)}) async-start(), calls=%async_computation.7 | async-start | bytes 655360 | tf_op jit(solution)/shard_map/reduce_scatter | solution.py:75
Sparse Core Ops, SparseCore 0:
  50.2 27.1 all-gather.1
  211.6 19.7 reduce-scatter.1
